TPU v7x, 32 devices: a whole 2x2x4 slice. The times are simulated.
32 devices in a mesh: ep: 4 (over y, x), tp: 8 (over z, core).
Axes of the slice: x: 2, y: 2, z: 4, core: 2. Of those that a mesh axis runs over, the one named last changes fastest.
Arguments:
- pool_input: bfloat16 [4096, 1024], P('ep', 'tp'), may hold values from -6 to 6
- pool_gain: float32 [1024], P('tp'), may hold values from 0.1 to 1.9
- mix_weight: bfloat16 [1024, 2048], P('tp'), may hold values from -0.1875 to 0.1875
- moe_input: bfloat16 [8192, 2048], P(('ep', 'tp')), may hold values from -6 to 6
- moe_gain: float32 [2048], replicated, may hold values from 0.1 to 1.9
- expert_ids: int32 [8192, 2], P(('ep', 'tp')), may hold values from 0 to 15, as said below
- route_weight: float32 [8192, 2], P(('ep', 'tp')), may hold values from 0.2 to 1
- gate_weight: bfloat16 [16, 2048, 1024], P('ep', None, 'tp'), may hold values from -0.125 to 0.125
- up_weight: bfloat16 [16, 2048, 1024], P('ep', None, 'tp'), may hold values from -0.125 to 0.125
- down_weight: bfloat16 [16, 2048, 1024], P('ep', None, 'tp'), may hold values from -0.1875 to 0.1875
Outputs:
- mixed_out: bfloat16 [4096, 2048], P(('ep', 'tp'))
- moe_out: bfloat16 [8192, 2048], P(('ep', 'tp'))
Inputs may be any that keep to these rules, and one draw needn't show every extreme that they name: `expert_ids`: each row names 2 different experts of one group of 4 consecutive experts. In each aligned block of 256 rows (the rows of one device) no expert is named by more than 48 rows, and some expert is named by exactly 48 rows.
All inputs are finite; a program needn't handle non-finite values.
Results may differ from a plain program's by a relative error of at most 0.012.
Values may be sent and summed in bfloat16 or wider, within the bound.
A program may use at most 128 MiB of HBM per device.

v0:
```python
import jax
import jax.numpy as jnp
from jax import lax
from jax.sharding import PartitionSpec as P

GROUP_CH = 256
EXPERTS = 16
TOP = 2
CAP = 48
eps_norm = 1e-06


def from_behind(shard, axis, by):
    peers = lax.axis_size(axis)
    pairs = [(i, i + by) for i in range(peers) if 0 <= i + by < peers]
    return lax.ppermute(shard, axis, pairs)


def window_sums(extended, row_count):
    level_sum = extended
    stride = 1
    outputs = []
    for doubling in range(4):
        level_sum = level_sum[stride:] + level_sum[:-stride]
        stride = stride * 2
        outputs.append(level_sum[level_sum.shape[0] - row_count :])
    return outputs


def pool_mixer(pool_input, pool_gain):
    row_count, channels = pool_input.shape
    carried = from_behind(pool_input[row_count - 15 :], "ep", 1)
    extended = jnp.concatenate([carried, pool_input], axis=0).astype(jnp.float32)
    window_list = window_sums(extended, row_count)
    channel_ids = lax.axis_index("tp") * channels + lax.iota(jnp.int32, channels)
    group_ids = channel_ids // GROUP_CH
    position = lax.axis_index("ep") * row_count + lax.iota(jnp.int32, row_count)
    summed = jnp.zeros((row_count, channels), jnp.float32)
    widths = jnp.zeros((channels,), jnp.int32)
    for index_group in range(4):
        inside = group_ids == index_group
        summed = jnp.where(inside[None, :], window_list[index_group], summed)
        widths = jnp.where(inside, 2 ** (index_group + 1), widths)
    counted = jnp.minimum(position[:, None] + 1, widths[None, :]).astype(jnp.float32)
    values = extended[15:]
    return ((summed / counted - values) * pool_gain).astype(jnp.bfloat16)


def route_slots(expert_ids):
    flat_ids = expert_ids.reshape(-1)
    marked = (flat_ids[:, None] == lax.iota(jnp.int32, EXPERTS)[None, :]).astype(jnp.int32)
    before_count = jnp.cumsum(marked, axis=0) - marked
    ranked = jnp.sum(before_count * marked, axis=1)
    return (flat_ids * CAP + ranked).reshape(expert_ids.shape)


def body(
    pool_input,
    pool_gain,
    mix_weight,
    moe_input,
    moe_gain,
    expert_ids,
    route_weight,
    gate_weight,
    up_weight,
    down_weight,
):
    pooled = pool_mixer(pool_input, pool_gain)
    regrouped = lax.all_to_all(pooled, "tp", split_axis=0, concat_axis=1, tiled=True)
    mixed_sum = jnp.dot(
        regrouped,
        lax.all_gather(mix_weight, "tp", axis=0, tiled=True),
        preferred_element_type=jnp.float32,
    )
    mixed_out = mixed_sum.astype(jnp.bfloat16)
    inputs = moe_input.astype(jnp.float32)
    scale_rows = lax.rsqrt(jnp.mean(inputs * inputs, axis=-1, keepdims=True) + eps_norm)
    normed = (inputs * scale_rows * moe_gain).astype(jnp.bfloat16)
    slots = route_slots(expert_ids)
    slot_index = lax.iota(jnp.int32, EXPERTS * CAP)
    placing = (
        (slot_index[:, None] == slots[None, :, 0]) | (slot_index[:, None] == slots[None, :, 1])
    ).astype(jnp.bfloat16)
    outgoing = jnp.dot(placing, normed, preferred_element_type=jnp.float32).astype(jnp.bfloat16)
    outgoing = outgoing.reshape(EXPERTS, CAP, normed.shape[1])
    arrived = lax.all_to_all(outgoing, "ep", split_axis=0, concat_axis=1, tiled=True)
    gate_piece = lax.all_gather(gate_weight, "tp", axis=2, tiled=True)
    up_piece = lax.all_gather(up_weight, "tp", axis=2, tiled=True)
    down_piece = lax.all_gather(down_weight, "tp", axis=2, tiled=True)
    gate_part = jnp.einsum("erd,edf->erf", arrived, gate_piece, preferred_element_type=jnp.float32)
    upward = jnp.einsum("erd,edf->erf", arrived, up_piece, preferred_element_type=jnp.float32)
    hidden = (jax.nn.silu(gate_part) * upward).astype(jnp.bfloat16)
    expert_sum = jnp.einsum("erf,edf->erd", hidden, down_piece, preferred_element_type=jnp.float32)
    expert_rows = expert_sum.astype(jnp.bfloat16)
    returned = lax.all_to_all(expert_rows, "ep", split_axis=1, concat_axis=0, tiled=True)
    returned_rows = returned.reshape(EXPERTS * CAP, returned.shape[2])
    combined = jnp.zeros((normed.shape[0], normed.shape[1]), jnp.float32)
    for route_index in range(TOP):
        picking = (slots[:, route_index][:, None] == slot_index[None, :]).astype(jnp.bfloat16)
        chosen_rows = jnp.dot(picking, returned_rows, preferred_element_type=jnp.float32)
        combined = combined + route_weight[:, route_index : route_index + 1] * chosen_rows
    moe_out = combined.astype(jnp.bfloat16)
    return (mixed_out, moe_out)


def solution(mesh):
    return jax.shard_map(
        body,
        mesh=mesh,
        in_specs=(
            P("ep", "tp"),
            P("tp"),
            P("tp", None),
            P(("ep", "tp"), None),
            P(),
            P(("ep", "tp"), None),
            P(("ep", "tp"), None),
            P("ep", None, "tp"),
            P("ep", None, "tp"),
            P("ep", None, "tp"),
        ),
        out_specs=(P(("ep", "tp"), None), P(("ep", "tp"), None)),
        check_vma=False,
    )
```

profile of v0, /device:TPU:0, one launch (start us, length us, event | category | flops | bytes accessed | tf_op | source)
XLA Modules:
  0.0 554.3 jit_solution(15557223583954882724)
XLA Ops:
  7.2 0.0 copy-start.5
  7.2 0.0 all-gather.7.cloned.1.call-start
  7.2 0.7 all-gather.7.cloned.1.call-update
  7.9 0.0 all-gather.11.cloned.1.call-start
  8.0 0.7 all-gather.11.cloned.1.call-update
  8.7 0.0 all-gather.9.cloned.1.call-start
  8.7 0.7 all-gather.9.cloned.1.call-update
  9.4 0.1 copy.47
  9.6 0.1 eq.138
  9.7 0.1 eq.134
  9.9 1.2 reduce-window.6
  11.0 0.2 slice_reduce_fusion
  11.3 0.1 fusion.23
  11.4 0.1 reduce_sum.21
  11.5 0.1 copy.50
  11.6 0.3 fusion.2
  11.9 0.0 copy-done.4
  12.0 2.8 convolution_convert_fusion
  14.7 5.3 all-to-all-start.1
  20.1 0.0 copy-done.3
  20.1 3.9 collective-permute-start
  24.0 0.0 all-gather.5.cloned.1.call-update
  24.1 30.0 %collective-permute-done = bf16[15,128]{1,0:T(8,128)(2,1)S(1)} collective-permute-done((bf16[15,128]{1,0:T(8,128)(2,1)S(1)}, bf16[15,128]{1,0:T(8,128)(2,1)S(1)}, u32[]{:S(2)}, u32[]{:S(2)}) %collective-permute-start) | collective-permute-done | bytes 3872 | tf_op jit(solution)/shard_map/ppermute | solution.py:16
  54.1 0.1 maximum_convert_fusion
  54.2 0.1 slice_add_fusion.1
  54.2 0.1 slice_add_fusion
  54.3 0.1 slice_add_fusion.2
  54.4 1.1 fusion.12
  55.4 0.8 all-to-all-done.1
  56.2 5.2 all-to-all-start
  61.4 1.9 copy.51
  63.3 107.9 %all-gather.7.cloned.1.call-done = bf16[4,2048,1024]{2,1,0:T(8,128)(2,1)} async-done(((bf16[4,2048,128]{2,1,0:T(8,128)(2,1)}), bf16[4,2048,1024]{2,1,0:T(8,128)(2,1)}) %all-gather.7.cloned.1.call-update) | async-done | bytes 16777232 | tf_op jit(solution)/shard_map/all_gather | solution.py:88
  171.2 11.9 %fusion.28 = f32[4,192,1024]{2,1,0:T(8,128)} fusion(bf16[4,192,2048]{2,1,0:T(8,128)(2,1)} %bitcast.48, bf16[4,2048,1024]{2,1,0:T(8,128)(2,1)} %all-gather.7.cloned.1.call-done), kind=kOutput, calls=%fused_computation.62 | convolution fusion | flops 3221225472 | bytes 23068672 | tf_op jit(solution)/shard_map/erd,edf->erf/dot_general | solution.py:91
  183.2 142.6 %all-gather.11.cloned.1.call-done = bf16[4,2048,1024]{2,1,0:T(8,128)(2,1)} async-done(((bf16[4,2048,128]{2,1,0:T(8,128)(2,1)}), bf16[4,2048,1024]{2,1,0:T(8,128)(2,1)}) %all-gather.11.cloned.1.call-update) | async-done | bytes 16777232 | tf_op jit(solution)/shard_map/all_gather | solution.py:90
  325.8 151.6 %all-gather.9.cloned.1.call-done = bf16[4,2048,1024]{2,1,0:T(8,128)(2,1)} async-done(((bf16[4,2048,128]{2,1,0:T(8,128)(2,1)}), bf16[4,2048,1024]{2,1,0:T(8,128)(2,1)}) %all-gather.9.cloned.1.call-update) | async-done | bytes 16777232 | tf_op jit(solution)/shard_map/all_gather | solution.py:89
  477.4 17.7 %convolution_convert_fusion.1 = bf16[4,192,2048]{2,1,0:T(8,128)(2,1)} fusion(bf16[4,2048,1024]{2,1,0:T(8,128)(2,1)} %all-gather.11.cloned.1.call-done, f32[4,192,1024]{2,1,0:T(8,128)} %fusion.28, bf16[4,192,2048]{2,1,0:T(8,128)(2,1)S(1)} %bitcast.49, bf16[4,2048,1024]{2,1,0:T(8,128)(2,1)} %all-gather.9.cloned.1.call-done), kind=kOutput, calls=%fused_computation.1 | convolution fusion | flops 6448742400 | bytes 42991616 | tf_op jit(solution)/shard_map/erf,edf->erd/dot_general | solution.py:94
  495.1 6.0 %copy.52 = bf16[4,192,2048]{2,0,1:T(4,128)(2,1)} copy(bf16[4,192,2048]{2,1,0:T(8,128)(2,1)} %convolution_convert_fusion.1) | data formatting | bytes 6291456 | tf_op jit(solution)/shard_map/convert_element_type | solution.py:95
  501.1 0.0 all-to-all-done
  501.1 0.7 copy-done.2
  501.8 3.9 all-to-all-start.2
  505.7 1.1 copy.46
  506.9 17.0 %all-gather.5.cloned.1.call-done = bf16[1024,2048]{1,0:T(8,128)(2,1)} async-done(((bf16[128,2048]{1,0:T(8,128)(2,1)}), bf16[1024,2048]{1,0:T(8,128)(2,1)}) %all-gather.5.cloned.1.call-update) | async-done | bytes 4194320 | tf_op jit(solution)/shard_map/all_gather | solution.py:73
  523.9 3.7 convolution_convert_fusion.2
  527.6 14.8 %all-to-all-done.2 = bf16[4,192,2048]{2,0,1:T(4,128)(2,1)S(1)} async-done(((bf16[4,192,2048]{2,0,1:T(4,128)(2,1)}), bf16[4,192,2048]{2,0,1:T(4,128)(2,1)S(1)}, u32[]{:S(2)}, u32[]{:S(2)}) %all-to-all-start.2) | async-done | bytes 3145760 | tf_op jit(solution)/shard_map/all_to_all | solution.py:96
  542.5 1.7 copy.53
  544.2 0.4 copy.54
  544.6 1.0 convolution_multiply_fusion.1
  545.7 2.1 fusion.1
  (25 shorter events, 0.1 us)
Async XLA Ops:
  7.2 2.3 copy-start.5
  7.2 4.4 copy-start.1
  7.2 164.1 %all-gather.7.cloned.1.call-start = ((), (), s32[]{:S(2)}) async-start(), calls=%async_computation.4 | async-start | bytes 18874368 | tf_op jit(solution)/shard_map/all_gather | solution.py:88
  7.9 4.0 copy-start.4
  7.9 317.8 %all-gather.11.cloned.1.call-start = ((), (), s32[]{:S(2)}) async-start(), calls=%async_computation.6 | async-start | bytes 18874368 | tf_op jit(solution)/shard_map/all_gather | solution.py:90
  8.7 468.7 %all-gather.9.cloned.1.call-start = ((), (), s32[]{:S(2)}) async-start(), calls=%async_computation.5 | async-start | bytes 18874368 | tf_op jit(solution)/shard_map/all_gather | solution.py:89
  14.7 5.3 copy-start.3
  14.7 41.5 %all-to-all-start.1 = ((bf16[16,48,2048]{2,1,0:T(8,128)(2,1)}), bf16[16,48,2048]{2,1,0:T(8,128)(2,1)S(1)}, u32[]{:S(2)}, u32[]{:S(2)}) async-start(bf16[16,48,2048]{2,1,0:T(8,128)(2,1)} %bitcast.7), calls=%async_computation.1 | async-start | bytes 6291456 | tf_op jit(solution)/shard_map/all_to_all | solution.py:87
  20.0 34.3 %copy-start.7 = (f32[128]{0:T(128)S(1)}, f32[128]{0:T(128)}, u32[]{:S(2)}) copy-start(f32[128]{0:T(128)} %param.11) | copy-start | bytes 1540
  20.0 503.9 %all-gather.5.cloned.1.call-start = ((), (), s32[]{:S(2)}) async-start(), calls=%async_computation.3 | async-start | bytes 4718592 | tf_op jit(solution)/shard_map/all_gather | solution.py:73
  20.1 34.0 %collective-permute-start = (bf16[15,128]{1,0:T(8,128)(2,1)S(1)}, bf16[15,128]{1,0:T(8,128)(2,1)S(1)}, u32[]{:S(2)}, u32[]{:S(2)}) collective-permute-start(bf16[15,128]{1,0:T(8,128)(2,1)S(1)} %slice.57), channel_id=1, source_target_pairs={{0,8},{8,16},{16,24},{1,9},{9,17},{17,25},{2,10},{10,18},{18,26},{... | collective-permute-start | bytes 11528 | tf_op jit(solution)/shard_map/ppermute | solution.py:16
  56.2 444.9 %all-to-all-start = ((bf16[8,128,128]{2,1,0:T(8,128)(2,1)}), bf16[8,128,128]{2,1,0:T(8,128)(2,1)S(1)}, u32[]{:S(2)}, u32[]{:S(2)}) async-start(bf16[8,128,128]{2,1,0:T(8,128)(2,1)} %bitcast), calls=%async_computation | async-start | bytes 524288 | tf_op jit(solution)/shard_map/all_to_all | solution.py:70
  171.2 306.1 %copy-start = (bf16[4,4,48,2048]{3,2,0,1:T(8,128)(2,1)S(1)}, bf16[4,4,48,2048]{3,2,0,1:T(8,128)(2,1)}, u32[]{:S(2)}) copy-start(bf16[4,4,48,2048]{3,2,0,1:T(8,128)(2,1)} %copy.51) | copy-start | bytes 9437188
  501.1 4.6 copy-start.6
  501.1 0.7 copy-start.2
  501.8 40.6 %all-to-all-start.2 = ((bf16[4,192,2048]{2,0,1:T(4,128)(2,1)}), bf16[4,192,2048]{2,0,1:T(4,128)(2,1)S(1)}, u32[]{:S(2)}, u32[]{:S(2)}) async-start(bf16[4,192,2048]{2,0,1:T(4,128)(2,1)} %copy.52), calls=%async_computation.2 | async-start | bytes 6291456 | tf_op jit(solution)/shard_map/all_to_all | solution.py:96
Sparse Core Ops, SparseCore 0:
  9.6 161.6 all-gather.6
  172.8 152.8 all-gather.10
  327.4 149.9 all-gather.8
  478.8 45.0 all-gather.4
where the time goes:
time: 555 us; the launch traced here: 554 us
  waiting for transfers between devices  467 us (84%)
  matrix products  39.2 us (7%)
  starting transfers between devices  18.4 us (3%)
  between operations  14 us (3%)
  local copies, waits for them, and re-layouts  12.8 us (2%)
    all_gather x1, waiting for transfers between devices, body(): up_piece = lax.all_gather(up_weight, 'tp', axis=2, tiled=True)  152 us
    all_gather x1, waiting for transfers between devices, body(): down_piece = lax.all_gather(down_weight, 'tp', axis=2, tiled=True)  143 us
    all_gather x1, waiting for transfers between devices, body(): gate_piece = lax.all_gather(gate_weight, 'tp', axis=2, tiled=True)  108 us
    ppermute x1, waiting for transfers between devices, from_behind(): return lax.ppermute(shard, axis, pairs)  30 us
    dot_general x1, matrix products, body(): jnp.einsum('erf,edf->erd', hidden, down_piece, preferred_element_type=jnp...  17.7 us
    all_gather x1, waiting for transfers between devices, body(): lax.all_gather(mix_weight, 'tp', axis=0, tiled=True)  17 us
    all_to_all x1, waiting for transfers between devices, body(): lax.all_to_all(expert_rows, 'ep', split_axis=1, concat_axis=0, tiled=True)  14.8 us
    dot_general x1, matrix products, body(): jnp.einsum('erd,edf->erf', arrived, gate_piece, preferred_element_type=jn...  11.9 us
  transfers between devices with their start and end apart: 8, of which 7 were waited for; matrix products, arithmetic and copies ran while one was open for 9% of the time, Pallas kernels for 0%

commit v1 on v0

--- a/solution.py
+++ b/solution.py
@@ -87,11 +87,40 @@
     arrived = lax.all_to_all(outgoing, "ep", split_axis=0, concat_axis=1, tiled=True)
     gate_piece = lax.all_gather(gate_weight, "tp", axis=2, tiled=True)
     up_piece = lax.all_gather(up_weight, "tp", axis=2, tiled=True)
-    down_piece = lax.all_gather(down_weight, "tp", axis=2, tiled=True)
     gate_part = jnp.einsum("erd,edf->erf", arrived, gate_piece, preferred_element_type=jnp.float32)
     upward = jnp.einsum("erd,edf->erf", arrived, up_piece, preferred_element_type=jnp.float32)
     hidden = (jax.nn.silu(gate_part) * upward).astype(jnp.bfloat16)
-    expert_sum = jnp.einsum("erf,edf->erd", hidden, down_piece, preferred_element_type=jnp.float32)
+    size, index, rows = (lax.axis_size("tp"), lax.axis_index("tp"), down_weight.shape[2])
+    right = [(i_2, (i_2 + 1) % size) for i_2 in range(size)]
+    backward = [(i_2, (i_2 - 1) % size) for i_2 in range(size)]
+    middle = size // 2
+    from_left = from_right = down_weight
+    expert_sum = jnp.einsum(
+        "erf,edf->erd",
+        lax.dynamic_slice_in_dim(hidden, index * rows, down_weight.shape[2], axis=2),
+        down_weight,
+        preferred_element_type=jnp.float32,
+    )
+    for step in range(1, middle + 1):
+        from_left = lax.ppermute(from_left, "tp", right)
+        if step < size - middle:
+            from_right = lax.ppermute(from_right, "tp", backward)
+            expert_sum = expert_sum + jnp.einsum(
+                "erf,edf->erd",
+                lax.dynamic_slice_in_dim(
+                    hidden, (index + step) % size * rows, from_right.shape[2], axis=2
+                ),
+                from_right,
+                preferred_element_type=jnp.float32,
+            )
+        expert_sum = expert_sum + jnp.einsum(
+            "erf,edf->erd",
+            lax.dynamic_slice_in_dim(
+                hidden, (index - step) % size * rows, from_left.shape[2], axis=2
+            ),
+            from_left,
+            preferred_element_type=jnp.float32,
+        )
     expert_rows = expert_sum.astype(jnp.bfloat16)
     returned = lax.all_to_all(expert_rows, "ep", split_axis=1, concat_axis=0, tiled=True)
     returned_rows = returned.reshape(EXPERTS * CAP, returned.shape[2])

time: 555 us -> 577 us (1.040)
  waiting for transfers between devices: 467 us -> 376 us
  starting transfers between devices: 18.4 us -> 81.8 us
  matrix products: 39.2 us -> 86 us
    ppermute x0 -> x7, waiting for transfers between devices: none -> 167 us  [the longest x4 167 us: body(): from_left = lax.ppermute(from_left, 'tp', right)]
    all_gather x1 -> x0, waiting for transfers between devices: 143 us -> none  [body(): down_piece = lax.all_gather(down_weight, 'tp', axis=2, tiled=True)]
    all_gather x1, waiting for transfers between devices: 108 us -> 13.4 us  [body(): gate_piece = lax.all_gather(gate_weight, 'tp', axis=2, tiled=True)]
    dot_general x1 -> x9, matrix products: 17.7 us -> 64.4 us  [the longest x4 32.4 us: body(): jnp.einsum('erf,edf->erd', lax.dynamic_slice_in_dim(hidden, (index - step...]
    all_to_all x1, starting transfers between devices: 5.19 us -> 48 us  [body(): lax.all_to_all(pooled, 'tp', split_axis=0, concat_axis=1, tiled=True)]
    ppermute x1, waiting for transfers between devices: 30 us -> 0.01 us  [from_behind(): return lax.ppermute(shard, axis, pairs)]
    ppermute x0 -> x7, starting transfers between devices: none -> 20.5 us  [the longest x3 10.5 us: body(): from_right = lax.ppermute(from_right, 'tp', backward)]
    all_gather x1, waiting for transfers between devices: 17 us -> 0.02 us  [body(): lax.all_gather(mix_weight, 'tp', axis=0, tiled=True)]
  transfers between devices with their start and end apart: 8 -> 14, of which waited for: 7 -> 6; matrix products, arithmetic and copies ran while one was open for 9% -> 16% of each run, Pallas kernels for 0% -> 0%
where the time goes in v1:
time: 577 us; the launch traced here: 572 us
  waiting for transfers between devices  376 us (65%)
  matrix products  86 us (15%)
  starting transfers between devices  81.8 us (14%)
  between operations  14.1 us (2%)
  local copies, waits for them, and re-layouts  10.9 us (2%)
    ppermute x4, waiting for transfers between devices, body(): from_left = lax.ppermute(from_left, 'tp', right)  167 us
    all_gather x1, waiting for transfers between devices, body(): up_piece = lax.all_gather(up_weight, 'tp', axis=2, tiled=True)  163 us
    all_to_all x1, starting transfers between devices, body(): lax.all_to_all(pooled, 'tp', split_axis=0, concat_axis=1, tiled=True)  48 us
    dot_general x4, matrix products, body(): jnp.einsum('erf,edf->erd', lax.dynamic_slice_in_dim(hidden, (index - step...  32.4 us
    all_to_all x1, waiting for transfers between devices, body(): lax.all_to_all(expert_rows, 'ep', split_axis=1, concat_axis=0, tiled=True)  31.6 us
    dot_general x3, matrix products, body(): jnp.einsum('erf,edf->erd', lax.dynamic_slice_in_dim(hidden, (index + step...  15.7 us
    all_gather x1, waiting for transfers between devices, body(): gate_piece = lax.all_gather(gate_weight, 'tp', axis=2, tiled=True)  13.4 us
    dot_general x1, matrix products, body(): jnp.einsum('erd,edf->erf', arrived, gate_piece, preferred_element_type=jn...  12 us
  transfers between devices with their start and end apart: 14, of which 6 were waited for; matrix products, arithmetic and copies ran while one was open for 16% of the time, Pallas kernels for 0%

profile of v1, /device:TPU:0, one launch (start us, length us, event | category | flops | bytes accessed | tf_op | source)
XLA Modules:
  0.0 571.9 jit_solution(1898352420636539814)
XLA Ops:
  7.2 0.7 all-gather.6.cloned.1.call-update
  8.0 0.7 all-gather.8.cloned.1.call-update
  8.7 0.5 collective-permute-start.2
  9.2 4.1 collective-permute-start.1
  13.3 74.5 %collective-permute-done.2 = bf16[4,2048,128]{2,1,0:T(8,128)(2,1)} collective-permute-done((bf16[4,2048,128]{2,1,0:T(8,128)(2,1)}, bf16[4,2048,128]{2,1,0:T(8,128)(2,1)}, u32[]{:S(2)}, u32[]{:S(2)}) %collective-permute-start.2) | collective-permute-done | bytes 2097184 | tf_op jit(solution)/shard_map/ppermute | solution.py:105
  87.9 0.7 collective-permute-start.4
  88.6 0.1 copy.47
  88.7 0.1 eq.146
  88.9 0.1 eq.142
  89.0 1.2 reduce-window.6
  90.2 0.2 slice_reduce_fusion
  90.4 0.1 fusion.37
  90.5 0.1 reduce_sum.21
  90.7 0.1 copy.50
  90.8 0.3 fusion.2
  91.1 2.8 convolution_convert_fusion
  93.9 5.2 all-to-all-start.1
  99.1 3.9 collective-permute-start
  103.1 2.9 collective-permute-start.3
  106.0 63.2 %collective-permute-done.4 = bf16[4,2048,128]{2,1,0:T(8,128)(2,1)} collective-permute-done((bf16[4,2048,128]{2,1,0:T(8,128)(2,1)}, bf16[4,2048,128]{2,1,0:T(8,128)(2,1)}, u32[]{:S(2)}, u32[]{:S(2)}) %collective-permute-start.4) | collective-permute-done | bytes 2097184 | tf_op jit(solution)/shard_map/ppermute | solution.py:105
  169.2 8.7 %collective-permute-start.6 = (bf16[4,2048,128]{2,1,0:T(8,128)(2,1)}, bf16[4,2048,128]{2,1,0:T(8,128)(2,1)}, u32[]{:S(2)}, u32[]{:S(2)}) collective-permute-start(bf16[4,2048,128]{2,1,0:T(8,128)(2,1)} %collective-permute-done.4), channel_id=1, source_target_pairs={{0,1},{1,2},{2,3},{3,4},{4,5},{5,6},{6,7},{7,0},{8,9},{9,10},{10,1... | collective-permute-start | bytes 6291464 | tf_op jit(solution)/shard_map/ppermute | solution.py:105
  178.3 1.1 fusion.11
  179.4 48.0 %all-to-all-start = ((bf16[8,128,128]{2,1,0:T(8,128)(2,1)}), bf16[8,128,128]{2,1,0:T(8,128)(2,1)S(1)}, u32[]{:S(2)}, u32[]{:S(2)}) async-start(bf16[8,128,128]{2,1,0:T(8,128)(2,1)} %bitcast), calls=%async_computation | async-start | bytes 524288 | tf_op jit(solution)/shard_map/all_to_all | solution.py:70
  227.4 1.9 copy.51
  229.3 3.5 collective-permute-start.5
  232.8 28.9 %collective-permute-done.6 = bf16[4,2048,128]{2,1,0:T(8,128)(2,1)} collective-permute-done((bf16[4,2048,128]{2,1,0:T(8,128)(2,1)}, bf16[4,2048,128]{2,1,0:T(8,128)(2,1)}, u32[]{:S(2)}, u32[]{:S(2)}) %collective-permute-start.6) | collective-permute-done | bytes 2097184 | tf_op jit(solution)/shard_map/ppermute | solution.py:105
  261.7 13.4 %all-gather.6.cloned.1.call-done = bf16[4,2048,1024]{2,1,0:T(8,128)(2,1)} async-done(((bf16[4,2048,128]{2,1,0:T(8,128)(2,1)}), bf16[4,2048,1024]{2,1,0:T(8,128)(2,1)}) %all-gather.6.cloned.1.call-update) | async-done | bytes 16777232 | tf_op jit(solution)/shard_map/all_gather | solution.py:88
  275.1 12.0 %fusion.49 = f32[4,192,1024]{2,1,0:T(8,128)} fusion(bf16[4,192,2048]{2,1,0:T(8,128)(2,1)} %bitcast.55, bf16[4,2048,1024]{2,1,0:T(8,128)(2,1)} %all-gather.6.cloned.1.call-done), kind=kOutput, calls=%fused_computation.83 | convolution fusion | flops 3221225472 | bytes 23068672 | tf_op jit(solution)/shard_map/erd,edf->erf/dot_general | solution.py:90
  287.1 163.1 %all-gather.8.cloned.1.call-done = bf16[4,2048,1024]{2,1,0:T(8,128)(2,1)} async-done(((bf16[4,2048,128]{2,1,0:T(8,128)(2,1)}), bf16[4,2048,1024]{2,1,0:T(8,128)(2,1)}) %all-gather.8.cloned.1.call-update) | async-done | bytes 16777232 | tf_op jit(solution)/shard_map/all_gather | solution.py:89
  450.3 10.4 %multiply_convert_fusion = bf16[4,192,1024]{2,1,0:T(8,128)(2,1)S(1)} fusion(f32[4,192,1024]{2,1,0:T(8,128)} %fusion.49, bf16[4,192,2048]{2,1,0:T(8,128)(2,1)S(1)} %bitcast.56, bf16[4,2048,1024]{2,1,0:T(8,128)(2,1)} %all-gather.8.cloned.1.call-done), kind=kOutput, calls=%fused_computation.2 | convolution fusion | flops 3225944064 | bytes 24641536 | tf_op jit(solution)/shard_map/erd,edf->erf/dot_general | solution.py:91
  460.7 5.9 %fusion.33 = f32[4,192,2048]{2,1,0:T(8,128)} fusion(bf16[4,2048,128]{2,1,0:T(8,128)(2,1)} %param.19, bf16[4,192,1024]{2,1,0:T(8,128)(2,1)S(1)} %multiply_convert_fusion, s32[]{:T(128)S(6)} %select_n.127), kind=kOutput, calls=%fused_computation.50 | convolution fusion | flops 402653184 | bytes 8585220 | tf_op jit(solution)/shard_map/erf,edf->erd/dot_general | solution.py:98
  466.6 5.2 fusion.25
  471.8 5.2 fusion.27
  477.1 5.2 fusion.29
  482.3 5.3 fusion.31
  487.5 5.2 fusion.21
  492.7 5.2 fusion.23
  497.9 16.8 %add_convert_fusion = bf16[4,192,2048]{2,1,0:T(8,128)(2,1)S(1)} fusion(f32[4,192,2048]{2,1,0:T(8,128)} %fusion.21, f32[4,192,2048]{2,1,0:T(8,128)} %fusion.23, f32[4,192,2048]{2,1,0:T(8,128)} %fusion.25, f32[4,192,2048]{2,1,0:T(8,128)} %fusion.27, f32[4,192,2048]{2,1,0:T(8,128)} %fusion.29, f32[4,192,2048]{2,1,0:T(8,128)} %fusion.33, ...), kind=kOutput, calls=%fused_computation | convolution fusion | flops 415236096 | bytes 49479684 | tf_op jit(solution)/shard_map/erf,edf->erd/dot_general | solution.py:116
  514.7 4.1 copy.52
  518.8 0.7 copy-done.3
  519.5 4.1 all-to-all-start.2
  523.7 1.1 copy.46
  524.8 3.7 convolution_convert_fusion.1
  528.5 31.6 %all-to-all-done.2 = bf16[4,192,2048]{2,0,1:T(4,128)(2,1)S(1)} async-done(((bf16[4,192,2048]{2,0,1:T(4,128)(2,1)}), bf16[4,192,2048]{2,0,1:T(4,128)(2,1)S(1)}, u32[]{:S(2)}, u32[]{:S(2)}) %all-to-all-start.2) | async-done | bytes 3145760 | tf_op jit(solution)/shard_map/all_to_all | solution.py:125
  560.1 1.7 copy.53
  561.8 0.4 copy.54
  562.3 1.0 convolution_multiply_fusion.1
  563.3 2.1 fusion.1
  (46 shorter events, 0.5 us)
Async XLA Ops:
  7.2 81.4 %copy-start.6 = (s32[256,2]{0,1:T(2,128)S(1)}, s32[256,2]{0,1:T(2,128)}, u32[]{:S(2)}) copy-start(s32[256,2]{0,1:T(2,128)} %param.15) | copy-start | bytes 6148
  7.2 83.6 %copy-start.1 = (bf16[256,2048]{1,0:T(8,128)(2,1)S(1)}, bf16[256,2048]{1,0:T(8,128)(2,1)}, u32[]{:S(2)}) copy-start(bf16[256,2048]{1,0:T(8,128)(2,1)} %param.13) | copy-start | bytes 3145732
  7.2 83.9 %copy-start.5 = (f32[2048]{0:T(1024)S(1)}, f32[2048]{0:T(1024)}, u32[]{:S(2)}) copy-start(f32[2048]{0:T(1024)} %param.14) | copy-start | bytes 24580
  7.2 268.0 %all-gather.6.cloned.1.call-start = ((), (), s32[]{:S(2)}) async-start(), calls=%async_computation.4 | async-start | bytes 18874368 | tf_op jit(solution)/shard_map/all_gather | solution.py:88
  7.9 442.3 %all-gather.8.cloned.1.call-start = ((), (), s32[]{:S(2)}) async-start(), calls=%async_computation.5 | async-start | bytes 18874368 | tf_op jit(solution)/shard_map/all_gather | solution.py:89
  8.7 79.2 %collective-permute-start.2 = (bf16[4,2048,128]{2,1,0:T(8,128)(2,1)}, bf16[4,2048,128]{2,1,0:T(8,128)(2,1)}, u32[]{:S(2)}, u32[]{:S(2)}) collective-permute-start(bf16[4,2048,128]{2,1,0:T(8,128)(2,1)} %param.19), channel_id=1, source_target_pairs={{0,1},{1,2},{2,3},{3,4},{4,5},{5,6},{6,7},{7,0},{8,9},{9,10},{10,1... | collective-permute-start | bytes 6291464 | tf_op jit(solution)/shard_map/ppermute | solution.py:105
  9.2 93.9 %collective-permute-start.1 = (bf16[4,2048,128]{2,1,0:T(8,128)(2,1)}, bf16[4,2048,128]{2,1,0:T(8,128)(2,1)}, u32[]{:S(2)}, u32[]{:S(2)}) collective-permute-start(bf16[4,2048,128]{2,1,0:T(8,128)(2,1)} %param.19), channel_id=1, source_target_pairs={{0,7},{1,0},{2,1},{3,2},{4,3},{5,4},{6,5},{7,6},{8,15},{9,8},{10,9... | collective-permute-start | bytes 6291464 | tf_op jit(solution)/shard_map/ppermute | solution.py:107
  87.9 81.3 %collective-permute-start.4 = (bf16[4,2048,128]{2,1,0:T(8,128)(2,1)}, bf16[4,2048,128]{2,1,0:T(8,128)(2,1)}, u32[]{:S(2)}, u32[]{:S(2)}) collective-permute-start(bf16[4,2048,128]{2,1,0:T(8,128)(2,1)} %collective-permute-done.2), channel_id=1, source_target_pairs={{0,1},{1,2},{2,3},{3,4},{4,5},{5,6},{6,7},{7,0},{8,9},{9,10},{10,1... | collective-permute-start | bytes 6291464 | tf_op jit(solution)/shard_map/ppermute | solution.py:105
  93.9 5.2 copy-start.4
  93.9 85.5 %all-to-all-start.1 = ((bf16[16,48,2048]{2,1,0:T(8,128)(2,1)}), bf16[16,48,2048]{2,1,0:T(8,128)(2,1)S(1)}, u32[]{:S(2)}, u32[]{:S(2)}) async-start(bf16[16,48,2048]{2,1,0:T(8,128)(2,1)} %bitcast.7), calls=%async_computation.1 | async-start | bytes 6291456 | tf_op jit(solution)/shard_map/all_to_all | solution.py:87
  99.1 425.8 %all-gather.4.cloned.1.call-start = ((), (), s32[]{:S(2)}) async-start(), calls=%async_computation.3 | async-start | bytes 4718592 | tf_op jit(solution)/shard_map/all_gather | solution.py:73
  99.1 79.2 %copy-start.8 = (f32[128]{0:T(128)S(1)}, f32[128]{0:T(128)}, u32[]{:S(2)}) copy-start(f32[128]{0:T(128)} %param.11) | copy-start | bytes 1540
  99.1 79.0 %collective-permute-start = (bf16[15,128]{1,0:T(8,128)(2,1)S(1)}, bf16[15,128]{1,0:T(8,128)(2,1)S(1)}, u32[]{:S(2)}, u32[]{:S(2)}) collective-permute-start(bf16[15,128]{1,0:T(8,128)(2,1)S(1)} %slice.57), channel_id=1, source_target_pairs={{0,8},{8,16},{16,24},{1,9},{9,17},{17,25},{2,10},{10,18},{18,26},{... | collective-permute-start | bytes 11528 | tf_op jit(solution)/shard_map/ppermute | solution.py:16
  103.1 126.2 %collective-permute-start.3 = (bf16[4,2048,128]{2,1,0:T(8,128)(2,1)}, bf16[4,2048,128]{2,1,0:T(8,128)(2,1)}, u32[]{:S(2)}, u32[]{:S(2)}) collective-permute-start(bf16[4,2048,128]{2,1,0:T(8,128)(2,1)} %collective-permute-done.1), channel_id=1, source_target_pairs={{0,7},{1,0},{2,1},{3,2},{4,3},{5,4},{6,5},{7,6},{8,15},{9,8},{10,9... | collective-permute-start | bytes 6291464 | tf_op jit(solution)/shard_map/ppermute | solution.py:107
  169.2 92.5 %collective-permute-start.6 = (bf16[4,2048,128]{2,1,0:T(8,128)(2,1)}, bf16[4,2048,128]{2,1,0:T(8,128)(2,1)}, u32[]{:S(2)}, u32[]{:S(2)}) collective-permute-start(bf16[4,2048,128]{2,1,0:T(8,128)(2,1)} %collective-permute-done.4), channel_id=1, source_target_pairs={{0,1},{1,2},{2,3},{3,4},{4,5},{5,6},{6,7},{7,0},{8,9},{9,10},{10,1... | collective-permute-start | bytes 6291464 | tf_op jit(solution)/shard_map/ppermute | solution.py:105
  179.4 339.4 %all-to-all-start = ((bf16[8,128,128]{2,1,0:T(8,128)(2,1)}), bf16[8,128,128]{2,1,0:T(8,128)(2,1)S(1)}, u32[]{:S(2)}, u32[]{:S(2)}) async-start(bf16[8,128,128]{2,1,0:T(8,128)(2,1)} %bitcast), calls=%async_computation | async-start | bytes 524288 | tf_op jit(solution)/shard_map/all_to_all | solution.py:70
  229.3 263.4 %collective-permute-start.5 = (bf16[4,2048,128]{2,1,0:T(8,128)(2,1)}, bf16[4,2048,128]{2,1,0:T(8,128)(2,1)}, u32[]{:S(2)}, u32[]{:S(2)}) collective-permute-start(bf16[4,2048,128]{2,1,0:T(8,128)(2,1)} %collective-permute-done.3), channel_id=1, source_target_pairs={{0,7},{1,0},{2,1},{3,2},{4,3},{5,4},{6,5},{7,6},{8,15},{9,8},{10,9... | collective-permute-start | bytes 6291464 | tf_op jit(solution)/shard_map/ppermute | solution.py:107
  261.7 236.2 %collective-permute-start.7 = (bf16[4,2048,128]{2,1,0:T(8,128)(2,1)}, bf16[4,2048,128]{2,1,0:T(8,128)(2,1)}, u32[]{:S(2)}, u32[]{:S(2)}) collective-permute-start(bf16[4,2048,128]{2,1,0:T(8,128)(2,1)} %collective-permute-done.6), channel_id=1, source_target_pairs={{0,1},{1,2},{2,3},{3,4},{4,5},{5,6},{6,7},{7,0},{8,9},{9,10},{10,1... | collective-permute-start | bytes 6291464 | tf_op jit(solution)/shard_map/ppermute | solution.py:105
  275.1 175.1 %copy-start = (bf16[4,4,48,2048]{3,2,0,1:T(8,128)(2,1)S(1)}, bf16[4,4,48,2048]{3,2,0,1:T(8,128)(2,1)}, u32[]{:S(2)}) copy-start(bf16[4,4,48,2048]{3,2,0,1:T(8,128)(2,1)} %copy.51) | copy-start | bytes 9437188
  460.7 32.0 %copy-start.2 = (bf16[4,192,1024]{2,1,0:T(8,128)(2,1)}, bf16[4,192,1024]{2,1,0:T(8,128)(2,1)S(1)}, u32[]{:S(2)}) copy-start(bf16[4,192,1024]{2,1,0:T(8,128)(2,1)S(1)} %multiply_convert_fusion) | copy-start | bytes 4718596
  518.8 4.9 copy-start.7
  518.8 0.7 copy-start.3
  519.5 40.6 %all-to-all-start.2 = ((bf16[4,192,2048]{2,0,1:T(4,128)(2,1)}), bf16[4,192,2048]{2,0,1:T(4,128)(2,1)S(1)}, u32[]{:S(2)}, u32[]{:S(2)}) async-start(bf16[4,192,2048]{2,0,1:T(4,128)(2,1)} %copy.52), calls=%async_computation.2 | async-start | bytes 6291456 | tf_op jit(solution)/shard_map/all_to_all | solution.py:125
Sparse Core Ops, SparseCore 0:
  9.6 265.5 all-gather.5
  276.7 173.4 all-gather.7
  451.9 53.2 all-gather.3
